TPU v7x, 256 devices: a whole 4x4x8 slice. The times are simulated.
256 devices in a mesh: sp: 16 (over y, x), tp: 16 (over z, core).
Axes of the slice: x: 4, y: 4, z: 8, core: 2. Of those that a mesh axis runs over, the one named last changes fastest.
Arguments:
- queries: bfloat16 [8192, 2048], P('sp', 'tp'), may hold values from -16 to 16
- key_vectors: bfloat16 [8192, 2048], P('sp', 'tp'), may hold values from -4 to 4
- value_vectors: bfloat16 [8192, 2048], P('sp', 'tp'), may hold values from -5 to 5
- forget_totals: float32 [8192, 16], P('sp', 'tp'), may hold values from -1368 to 0, as said below
- head_gain: float32 [2048], P('tp'), may hold values from 0.1 to 1.9
- stream: bfloat16 [8192, 2048], P(('sp', 'tp')), may hold values from -6 to 6
- out_weight: bfloat16 [2048, 2048], replicated, may hold values from -0.125 to 0.125
- norm_gain: float32 [2048], replicated, may hold values from 0.1 to 1.9
- routing: int32 [8192, 2], P(('sp', 'tp')), may hold values from 0 to 15, all different within a row; in each aligned block of 32 rows (0 to 31, 32 to 63, ...) at most 8 rows name the same one
- route_weights: float32 [8192, 2], P(('sp', 'tp')), may hold values from 0.2 to 1
- gate_weight: bfloat16 [16, 2048, 4096], P('sp', None, 'tp'), may hold values from -0.125 to 0.125
- up_weight: bfloat16 [16, 2048, 4096], P('sp', None, 'tp'), may hold values from -0.125 to 0.125
- down_weight: bfloat16 [16, 4096, 2048], P('sp', 'tp'), may hold values from -0.09375 to 0.09375
Outputs:
- layer_out: bfloat16 [8192, 2048], P(('sp', 'tp'))
Inputs may be any that keep to these rules, and one draw needn't show every extreme that they name: `forget_totals`: along the positions, the values of each head never rise. `routing`: A token's 2 experts differ. Within the tokens of one device (aligned blocks of 32 rows) no expert is named more than 8 times.
All inputs are finite; a program needn't handle non-finite values.
Results may differ from a plain program's by a relative error of at most 0.01145.
Values may be sent and summed in bfloat16 or wider, within the bound.
A program may use at most 128 MiB of HBM per device.

v0:
```python
from functools import partial
import jax
import jax.numpy as jnp
from jax import lax
from jax.sharding import PartitionSpec as P

HD = 128
TOP = 2
masked_score = -1e30


def sent_together(arrays, axis, dim, along):
    ends, at = ([], 0)
    for a in arrays[:-1]:
        at += a.shape[along]
        ends.append(at)
    both = jnp.concatenate(arrays, axis=along)
    return tuple(jnp.split(lax.all_gather(both, axis, axis=dim, tiled=True), ends, axis=along))


def attend_block(
    totals, query_rows, query_gate, query_pos, key_rows, value_rows, key_gate, key_pos
):
    run_max, run_sum, run_acc = totals
    scores = jnp.einsum("qhd,khd->hqk", query_rows, key_rows, preferred_element_type=jnp.float32)
    scores = scores * HD ** (-0.5) + query_gate[:, :, None] - key_gate[:, None, :]
    visible = (key_pos[None, :] <= query_pos[:, None])[None]
    scores = jnp.where(visible, scores, masked_score)
    new_max = jnp.maximum(run_max, jnp.max(scores, axis=2))
    lifted = jnp.where(visible, jnp.exp(scores - new_max[:, :, None]), 0.0)
    rescale = jnp.exp(run_max - new_max)
    new_sum = run_sum * rescale + jnp.sum(lifted, axis=2)
    product = jnp.einsum(
        "hqk,khd->hqd", lifted.astype(jnp.bfloat16), value_rows, preferred_element_type=jnp.float32
    )
    new_acc = run_acc * rescale[:, :, None] + product
    return (new_max, new_sum, new_acc)


def keep_totals(totals_in):
    return totals_in


def make_folder(segments, gathered_gates):

    def fold_keys(state_all, key_piece, first_key):
        key_part, value_part = key_piece
        key_total = key_part.shape[0]
        block_len = min(512, key_total)
        heads_dev = segments[0][0].shape[1]
        key_part = key_part.reshape(key_total, heads_dev, HD)
        value_part = value_part.reshape(key_total, heads_dev, HD)

        def one_block(block_index, state_now):
            offset = block_index * block_len
            key_rows = lax.dynamic_slice_in_dim(key_part, offset, block_len, 0)
            value_rows = lax.dynamic_slice_in_dim(value_part, offset, block_len, 0)
            key_pos = offset + jnp.arange(block_len, dtype=jnp.int32)
            key_gate = jnp.transpose(lax.dynamic_slice_in_dim(gathered_gates, offset, block_len, 0))
            updated = []
            for segment, totals_in in zip(segments, state_now):
                query_rows, query_gate, query_pos = segment
                needed = offset <= query_pos[-1]
                advance = partial(
                    attend_block,
                    query_rows=query_rows,
                    query_gate=query_gate,
                    query_pos=query_pos,
                    key_rows=key_rows,
                    value_rows=value_rows,
                    key_gate=key_gate,
                    key_pos=key_pos,
                )
                updated.append(lax.cond(needed, advance, keep_totals, totals_in))
            return tuple(updated)

        return lax.fori_loop(0, key_total // block_len, one_block, state_all)

    return fold_keys


def on_device(
    queries,
    key_vectors,
    value_vectors,
    forget_totals,
    head_gain,
    stream,
    out_weight,
    norm_gain,
    routing,
    route_weights,
    gate_weight,
    up_weight,
    down_weight,
):
    tok_count = queries.shape[0]
    heads_dev = queries.shape[1] // HD
    sp_index = lax.axis_index("sp")
    sp_count = lax.axis_size("sp")
    gathered_gates = lax.all_gather(forget_totals, "sp", axis=0, tiled=True)
    first_pos = sp_index * tok_count
    query_pos = first_pos + jnp.arange(tok_count, dtype=jnp.int32)
    query_gate = jnp.transpose(lax.dynamic_slice_in_dim(gathered_gates, first_pos, tok_count, 0))
    segments = [(queries.reshape(tok_count, heads_dev, HD), query_gate, query_pos)]
    starting = (
        (
            jnp.full((heads_dev, tok_count), masked_score, jnp.float32),
            jnp.zeros((heads_dev, tok_count), jnp.float32),
            jnp.zeros((heads_dev, tok_count, HD), jnp.float32),
        ),
    )
    folder = make_folder(segments, gathered_gates)
    totals = folder(starting, sent_together((key_vectors, value_vectors), "sp", 0, 1), jnp.int32(0))
    run_max, run_sum, run_acc = totals[0]
    attended = run_acc / run_sum[:, :, None]
    inverse_rms = lax.rsqrt(jnp.mean(attended * attended, axis=2, keepdims=True) + 1e-06)
    normed = attended * inverse_rms * head_gain.reshape(heads_dev, 1, HD)
    head_out = (
        jnp.transpose(normed, (1, 0, 2)).reshape(tok_count, heads_dev * HD).astype(jnp.bfloat16)
    )
    token_heads = lax.all_to_all(head_out, "tp", split_axis=0, concat_axis=1, tiled=True)
    mixed_rows = jnp.dot(token_heads, out_weight, preferred_element_type=jnp.float32)
    resid_sum = stream.astype(jnp.float32) + mixed_rows
    center = resid_sum - jnp.mean(resid_sum, axis=1, keepdims=True)
    normed_rows = (
        center * lax.rsqrt(jnp.mean(center * center, axis=1, keepdims=True) + 1e-05) * norm_gain
    ).astype(jnp.bfloat16)
    row_count = normed_rows.shape[0]
    capacity = max(2, 2 * TOP * row_count // sp_count)
    flat_expert = routing.reshape(-1)
    onehot = (flat_expert[:, None] == jnp.arange(sp_count, dtype=jnp.int32)[None, :]).astype(
        jnp.int32
    )
    earlier = jnp.cumsum(onehot, axis=0) - onehot
    slot_index = flat_expert * capacity + jnp.sum(earlier * onehot, axis=1)
    slot_grid = slot_index.reshape(row_count, TOP)
    slot_ids = jnp.arange(sp_count * capacity, dtype=jnp.int32)
    placing = jnp.sum(
        (slot_grid[None, :, :] == slot_ids[:, None, None]).astype(jnp.float32), axis=2
    ).astype(jnp.bfloat16)
    outgoing = jnp.dot(placing, normed_rows, preferred_element_type=jnp.float32).astype(
        jnp.bfloat16
    )
    outgoing = outgoing.reshape(sp_count, capacity, normed_rows.shape[1])
    arrived = lax.all_to_all(outgoing, "sp", split_axis=0, concat_axis=0, tiled=True)
    row_piece = lax.all_gather(arrived.reshape(-1, arrived.shape[2]), "tp", axis=0, tiled=True)
    gate_pre = jnp.dot(row_piece, gate_weight[0], preferred_element_type=jnp.float32)
    up_pre = jnp.dot(row_piece, up_weight[0], preferred_element_type=jnp.float32)
    hidden = (jax.nn.silu(gate_pre) * up_pre).astype(jnp.bfloat16)
    summed = lax.psum_scatter(
        jnp.dot(hidden, down_weight[0], preferred_element_type=jnp.float32).astype(jnp.bfloat16),
        "tp",
        scatter_dimension=0,
        tiled=True,
    )
    expert_out = summed.reshape(sp_count, capacity, -1)
    returned = lax.all_to_all(expert_out, "sp", split_axis=0, concat_axis=0, tiled=True)
    picked = returned.reshape(sp_count * capacity, -1)[slot_index].astype(jnp.float32)
    weighted = picked * route_weights.reshape(-1)[:, None]
    routed = jnp.sum(weighted.reshape(row_count, TOP, -1), axis=1)
    return (resid_sum + routed).astype(jnp.bfloat16)


def solution(mesh):
    in_specs = (
        P("sp", "tp"),
        P("sp", "tp"),
        P("sp", "tp"),
        P("sp", "tp"),
        P("tp"),
        P(("sp", "tp"), None),
        P(),
        P(),
        P(("sp", "tp"), None),
        P(("sp", "tp"), None),
        P("sp", None, "tp"),
        P("sp", None, "tp"),
        P("sp", "tp", None),
    )
    out_specs = P(("sp", "tp"), None)
    return jax.shard_map(
        on_device, mesh=mesh, in_specs=in_specs, out_specs=out_specs, check_vma=False
    )
```

profile of v0, /device:TPU:2, one launch (start us, length us, event | category | flops | bytes accessed | tf_op | source)
XLA Modules:
  0.0 334.1 jit_solution(2829663943095619503)
XLA Ops:
  6.5 1.8 pad_maximum_fusion
  8.3 0.8 copy.26
  9.7 23.4 %all_gather.10 = f32[8192,1]{0,1:T(1,128)S(1)} all-gather(f32[512,1]{0,1:T(1,128)} %param.20), channel_id=1, replica_groups=mesh['sp'=16,'tp'=16] {'sp'}, dimensions={0}, use_global_device_ids=true | all-gather | bytes 34816 | tf_op jit(solution)/shard_map/all_gather | solution.py:101
  33.1 36.1 %all-gather.3.cloned.1.call-done = bf16[8192,256]{1,0:T(8,128)(2,1)} async-done(((bf16[512,256]{1,0:T(8,128)(2,1)}), bf16[8192,256]{1,0:T(8,128)(2,1)}) %all-gather.3.cloned.1.call-update) | async-done | bytes 4194320 | tf_op jit(solution)/shard_map/all_gather | solution.py:18
  69.2 3.8 %slice_bitcast_fusion = (bf16[8192,1,128]{2,0,1:T(8,128)(2,1)S(1)}, bf16[8192,1,128]{2,0,1:T(8,128)(2,1)}) fusion(bf16[8192,256]{1,0:T(8,128)(2,1)} %all-gather.3.cloned.1.call-done), kind=kLoop, calls=%fused_computation.33 | loop fusion | bytes 8388608 | tf_op jit(solution)/shard_map/reshape | solution.py:52
  73.1 23.5 %while.17 = (s32[]{:T(128)}, f32[1,512]{1,0:T(1,128)S(1)}, f32[1,512]{1,0:T(1,128)S(1)}, f32[1,512,128]{2,1,0:T(8,128)S(1)}, s32[512]{0:T(512)S(1)}, /*index=5*/...) while((s32[]{:T(128)}, f32[1,512]{1,0:T(1,128)S(1)}, ...), condition=%wide.region_5.6_spmd, body=%wide.region_0.5_spmd.sunk | while | flops 138020352 | bytes 4122969 | solution.py:77
  74.3 2.2 conditional.2
  74.3 1.4 fusion.38
  77.7 2.2 conditional.2
  77.7 1.4 fusion.38
  96.8 0.9 multiply_convert_fusion.1
  97.7 7.1 %all-to-all-start = ((bf16[16,32,128]{2,1,0:T(8,128)(2,1)}), bf16[16,32,128]{2,1,0:T(8,128)(2,1)S(1)}, u32[]{:S(2)}, u32[]{:S(2)}) async-start(bf16[16,32,128]{2,1,0:T(8,128)(2,1)} %bitcast.16), calls=%async_computation | async-start | bytes 262144 | tf_op jit(solution)/shard_map/all_to_all | solution.py:122
  105.1 8.4 %all-to-all-done = bf16[16,32,128]{2,1,0:T(8,128)(2,1)S(1)} async-done(((bf16[16,32,128]{2,1,0:T(8,128)(2,1)}), bf16[16,32,128]{2,1,0:T(8,128)(2,1)S(1)}, u32[]{:S(2)}, u32[]{:S(2)}) %all-to-all-start) | async-done | bytes 131104 | tf_op jit(solution)/shard_map/all_to_all | solution.py:122
  113.5 5.0 %fusion.39 = (f32[32]{0:T(128)S(1)}, f32[32,2048]{1,0:T(8,128)S(1)}) fusion(bf16[2048,2048]{1,0:T(8,128)(2,1)} %param.23, bf16[32,2048]{1,0:T(8,128)(2,1)} %param.22, bf16[16,32,128]{2,1,0:T(8,128)(2,1)S(1)} %all-to-all-done), kind=kOutput, calls=%fused_computation.72 | convolution fusion | flops 268632032 | bytes 8913024 | tf_op jit(solution)/shard_map/dot_general | solution.py:123
  119.1 46.6 %all_to_all.26 = bf16[16,8,2048]{2,1,0:T(8,128)(2,1)} all-to-all(bf16[16,8,2048]{2,1,0:T(8,128)(2,1)S(1)} %fusion.21), channel_id=1, replica_groups=mesh['sp'=16,'tp'=16] {'sp'}, dimensions={0} | all-to-all | bytes 1048576 | tf_op jit(solution)/shard_map/all_to_all | solution.py:146
  165.8 49.9 %all-gather.5.cloned.1.call-done = bf16[2048,2048]{1,0:T(8,128)(2,1)} async-done(((bf16[128,2048]{1,0:T(8,128)(2,1)}), bf16[2048,2048]{1,0:T(8,128)(2,1)}) %all-gather.5.cloned.1.call-update) | async-done | bytes 8388624 | tf_op jit(solution)/shard_map/all_gather | solution.py:147
  215.8 7.1 %fusion.25 = f32[2048,256]{1,0:T(8,128)} fusion(bf16[2048,2048]{1,0:T(8,128)(2,1)} %all-gather.5.cloned.1.call-done, bf16[1,2048,256]{2,1,0:T(8,128)(2,1)S(1)} %copy-done.4), kind=kOutput, calls=%fused_computation.37 | convolution fusion | flops 2147483648 | bytes 11534336 | tf_op jit(solution)/shard_map/dot_general | solution.py:148
  222.9 16.8 %convolution_convert_fusion = bf16[2048,2048]{1,0:T(8,128)(2,1)} fusion(bf16[2048,2048]{1,0:T(8,128)(2,1)} %all-gather.5.cloned.1.call-done, f32[2048,256]{1,0:T(8,128)} %fusion.25, bf16[1,256,2048]{2,1,0:T(8,128)(2,1)S(1)} %copy-done, bf16[1,2048,256]{2,1,0:T(8,128)(2,1)} %param.28), kind=kOutput, calls=%fused_computation.27 | convolution fusion | flops 4302307328 | bytes 20971520 | tf_op jit(solution)/shard_map/dot_general | solution.py:152
  239.7 69.3 %reduce-scatter.2.cloned.1.call-done = bf16[128,2048]{1,0:T(8,128)(2,1)} async-done(((bf16[2048,2048]{1,0:T(8,128)(2,1)}), bf16[128,2048]{1,0:T(8,128)(2,1)}) %reduce-scatter.2.cloned.1.call-update) | async-done | bytes 524304 | tf_op jit(solution)/shard_map/reduce_scatter | solution.py:151
  309.0 7.3 %all-to-all-start.2 = ((bf16[16,8,2048]{2,1,0:T(8,128)(2,1)}), bf16[16,8,2048]{2,1,0:T(8,128)(2,1)S(1)}, u32[]{:S(2)}, u32[]{:S(2)}) async-start(bf16[16,8,2048]{2,1,0:T(8,128)(2,1)} %bitcast.76), calls=%async_computation.3 | async-start | bytes 1048576 | tf_op jit(solution)/shard_map/all_to_all | solution.py:158
  316.5 8.6 %all-to-all-done.2 = bf16[16,8,2048]{2,1,0:T(8,128)(2,1)S(1)} async-done(((bf16[16,8,2048]{2,1,0:T(8,128)(2,1)}), bf16[16,8,2048]{2,1,0:T(8,128)(2,1)S(1)}, u32[]{:S(2)}, u32[]{:S(2)}) %all-to-all-start.2) | async-done | bytes 524320 | tf_op jit(solution)/shard_map/all_to_all | solution.py:158
  325.1 0.7 gather_fusion
  326.2 0.7 multiply_reduce_fusion
  326.9 0.7 add_convert_fusion
  (100 shorter events, 13.3 us)
Async XLA Ops:
  6.5 216.3 %copy-start = (bf16[1,256,2048]{2,1,0:T(8,128)(2,1)S(1)}, bf16[1,256,2048]{2,1,0:T(8,128)(2,1)}, u32[]{:S(2)}) copy-start(bf16[1,256,2048]{2,1,0:T(8,128)(2,1)} %param.29) | copy-start | bytes 3145732
  6.5 62.7 %all-gather.3.cloned.1.call-start = ((), (), s32[]{:S(2)}) async-start(), calls=%async_computation.4 | async-start | bytes 4456448 | tf_op jit(solution)/shard_map/all_gather | solution.py:18
  73.1 23.8 %copy-start.3 = (f32[128]{0:T(128)S(1)}, f32[128]{0:T(128)}, u32[]{:S(2)}) copy-start(f32[128]{0:T(128)} %param.21) | copy-start | bytes 1540
  97.7 15.8 %all-to-all-start = ((bf16[16,32,128]{2,1,0:T(8,128)(2,1)}), bf16[16,32,128]{2,1,0:T(8,128)(2,1)S(1)}, u32[]{:S(2)}, u32[]{:S(2)}) async-start(bf16[16,32,128]{2,1,0:T(8,128)(2,1)} %bitcast.16), calls=%async_computation | async-start | bytes 262144 | tf_op jit(solution)/shard_map/all_to_all | solution.py:122
  104.8 110.9 %all-gather.5.cloned.1.call-start = ((), (), s32[]{:S(2)}) async-start(), calls=%async_computation.5 | async-start | bytes 8912896 | tf_op jit(solution)/shard_map/all_gather | solution.py:147
  105.1 13.7 %copy-start.1 = (f32[2048]{0:T(1024)S(1)}, f32[2048]{0:T(1024)}, u32[]{:S(2)}) copy-start(f32[2048]{0:T(1024)} %param.24) | copy-start | bytes 24580
  118.5 97.3 %copy-start.4 = (bf16[1,2048,256]{2,1,0:T(8,128)(2,1)S(1)}, bf16[1,2048,256]{2,1,0:T(8,128)(2,1)}, u32[]{:S(2)}) copy-start(bf16[1,2048,256]{2,1,0:T(8,128)(2,1)} %param.27) | copy-start | bytes 3145732
  165.8 143.2 %reduce-scatter.2.cloned.1.call-start = ((), (), s32[]{:S(2)}) async-start(), calls=%async_computation.6 | async-start | bytes 8912896 | tf_op jit(solution)/shard_map/reduce_scatter | solution.py:151
  239.7 76.8 %copy-start.2 = (f32[32,2]{0,1:T(2,128)S(1)}, f32[32,2]{0,1:T(2,128)}, u32[]{:S(2)}) copy-start(f32[32,2]{0,1:T(2,128)} %param.26) | copy-start | bytes 772
  309.0 16.1 %all-to-all-start.2 = ((bf16[16,8,2048]{2,1,0:T(8,128)(2,1)}), bf16[16,8,2048]{2,1,0:T(8,128)(2,1)S(1)}, u32[]{:S(2)}, u32[]{:S(2)}) async-start(bf16[16,8,2048]{2,1,0:T(8,128)(2,1)} %bitcast.76), calls=%async_computation.3 | async-start | bytes 1048576 | tf_op jit(solution)/shard_map/all_to_all | solution.py:158
Sparse Core Ops, SparseCore 0:
  9.8 59.4 all-gather.2
  165.9 49.8 all-gather.4
  239.8 69.1 reduce-scatter.1
where the time goes:
time: 335 us; the launch traced here: 334 us
  waiting for transfers between devices  172 us (51%)
  blocking collectives  70.1 us (21%)
  matrix products  33 us (10%)
  local copies, waits for them, and re-layouts  15.5 us (5%)
  starting transfers between devices  14.5 us (4%)
  between operations  13.3 us (4%)
  loops' own time  9.92 us (3%)
  other arithmetic  5.49 us (2%)
    reduce_scatter x1, waiting for transfers between devices, on_device(): lax.psum_scatter(jnp.dot(hidden, down_weight[0], preferred_element_type=j...  69.3 us
    all_gather x1, waiting for transfers between devices, on_device(): lax.all_gather(arrived.reshape(-1, arrived.shape[2]), 'tp', axis=0, tiled...  49.9 us
    all_to_all x1, blocking collectives, on_device(): lax.all_to_all(outgoing, 'sp', split_axis=0, concat_axis=0, tiled=True)  46.6 us
    all_gather x1, waiting for transfers between devices, sent_together(): lax.all_gather(both, axis, axis=dim, tiled=True)  36.1 us
    all_gather x1, blocking collectives, on_device(): gathered_gates = lax.all_gather(forget_totals, 'sp', axis=0, tiled=True)  23.4 us
    dot_general x1, matrix products, on_device(): jnp.dot(hidden, down_weight[0], preferred_element_type=jnp.float32)  16.8 us
    another operation x1, loops' own time, fold_keys(): return lax.fori_loop(0, key_total // block_len, one_block, state_all)  9.6 us
    slice x16, local copies, waits for them, and re-layouts, one_block(): needed = offset <= query_pos[-1]  9.2 us
  transfers between devices with their start and end apart: 5, of which 5 were waited for; matrix products, arithmetic and copies ran while one was open for 1% of the time, Pallas kernels for 0%

commit v1 on v0

--- a/solution.py
+++ b/solution.py
@@ -144,7 +144,9 @@
     )
     outgoing = outgoing.reshape(sp_count, capacity, normed_rows.shape[1])
     arrived = lax.all_to_all(outgoing, "sp", split_axis=0, concat_axis=0, tiled=True)
-    row_piece = lax.all_gather(arrived.reshape(-1, arrived.shape[2]), "tp", axis=0, tiled=True)
+    array = arrived.reshape(-1, arrived.shape[2])
+    copies = jnp.concatenate([array] * lax.axis_size("tp"), axis=0)
+    row_piece = lax.all_to_all(copies, "tp", 0, 0, tiled=True)
     gate_pre = jnp.dot(row_piece, gate_weight[0], preferred_element_type=jnp.float32)
     up_pre = jnp.dot(row_piece, up_weight[0], preferred_element_type=jnp.float32)
     hidden = (jax.nn.silu(gate_pre) * up_pre).astype(jnp.bfloat16)

time: 335 us -> 471 us (1.41)
  blocking collectives: 70.1 us -> 257 us
  waiting for transfers between devices: 172 us -> 120 us
    all_to_all x0 -> x1, blocking collectives: none -> 187 us  [on_device(): row_piece = lax.all_to_all(copies, 'tp', 0, 0, tiled=True)]
    all_gather x1 -> x0, waiting for transfers between devices: 49.9 us -> none  [on_device(): lax.all_gather(arrived.reshape(-1, arrived.shape[2]), 'tp', axis=0, tiled...]
  transfers between devices with their start and end apart: 5 -> 4, of which waited for: 5 -> 4; matrix products, arithmetic and copies ran while one was open for 1% -> 0% of each run, Pallas kernels for 0% -> 0%
where the time goes in v1:
time: 471 us; the launch traced here: 470 us
  blocking collectives  257 us (55%)
  waiting for transfers between devices  120 us (25%)
  matrix products  29.8 us (6%)
  local copies, waits for them, and re-layouts  19.3 us (4%)
  starting transfers between devices  14.4 us (3%)
  between operations  13.7 us (3%)
  loops' own time  9.92 us (2%)
  other arithmetic  5.5 us (1%)
    all_to_all x1, blocking collectives, on_device(): row_piece = lax.all_to_all(copies, 'tp', 0, 0, tiled=True)  187 us
    reduce_scatter x1, waiting for transfers between devices, on_device(): lax.psum_scatter(jnp.dot(hidden, down_weight[0], preferred_element_type=j...  66.7 us
    all_to_all x1, blocking collectives, on_device(): lax.all_to_all(outgoing, 'sp', split_axis=0, concat_axis=0, tiled=True)  46.6 us
    all_gather x1, waiting for transfers between devices, sent_together(): lax.all_gather(both, axis, axis=dim, tiled=True)  36.1 us
    all_gather x1, blocking collectives, on_device(): gathered_gates = lax.all_gather(forget_totals, 'sp', axis=0, tiled=True)  23.4 us
    dot_general x1, matrix products, on_device(): jnp.dot(hidden, down_weight[0], preferred_element_type=jnp.float32)  16.8 us
    another operation x1, loops' own time, fold_keys(): return lax.fori_loop(0, key_total // block_len, one_block, state_all)  9.6 us
  transfers between devices with their start and end apart: 4, of which 4 were waited for; matrix products, arithmetic and copies ran while one was open for 0% of the time, Pallas kernels for 0%

profile of v1, /device:TPU:2, one launch (start us, length us, event | category | flops | bytes accessed | tf_op | source)
XLA Modules:
  0.0 469.7 jit_solution(1226308253965401262)
XLA Ops:
  6.5 1.8 pad_maximum_fusion
  8.3 0.8 copy.26
  9.7 23.4 %all_gather.7 = f32[8192,1]{0,1:T(1,128)S(1)} all-gather(f32[512,1]{0,1:T(1,128)} %param.20), channel_id=1, replica_groups=mesh['sp'=16,'tp'=16] {'sp'}, dimensions={0}, use_global_device_ids=true | all-gather | bytes 34816 | tf_op jit(solution)/shard_map/all_gather | solution.py:101
  33.1 36.1 %all-gather.2.cloned.1.call-done = bf16[8192,256]{1,0:T(8,128)(2,1)} async-done(((bf16[512,256]{1,0:T(8,128)(2,1)}), bf16[8192,256]{1,0:T(8,128)(2,1)}) %all-gather.2.cloned.1.call-update) | async-done | bytes 4194320 | tf_op jit(solution)/shard_map/all_gather | solution.py:18
  69.2 3.8 slice_bitcast_fusion
  73.1 23.5 %while.17 = (s32[]{:T(128)}, f32[1,512]{1,0:T(1,128)S(1)}, f32[1,512]{1,0:T(1,128)S(1)}, f32[1,512,128]{2,1,0:T(8,128)S(1)}, s32[512]{0:T(512)S(1)}, /*index=5*/...) while((s32[]{:T(128)}, f32[1,512]{1,0:T(1,128)S(1)}, ...), condition=%wide.region_5.6_spmd, body=%wide.region_0.5_spmd.sunk | while | flops 138020352 | bytes 4122969 | solution.py:77
  74.3 2.2 conditional.2
  74.3 1.4 fusion.38
  77.7 2.2 conditional.2
  77.7 1.4 fusion.38
  96.8 0.9 multiply_convert_fusion.1
  97.7 7.1 %all-to-all-start = ((bf16[16,32,128]{2,1,0:T(8,128)(2,1)}), bf16[16,32,128]{2,1,0:T(8,128)(2,1)S(1)}, u32[]{:S(2)}, u32[]{:S(2)}) async-start(bf16[16,32,128]{2,1,0:T(8,128)(2,1)} %bitcast.16), calls=%async_computation | async-start | bytes 262144 | tf_op jit(solution)/shard_map/all_to_all | solution.py:122
  105.1 8.4 %all-to-all-done = bf16[16,32,128]{2,1,0:T(8,128)(2,1)S(1)} async-done(((bf16[16,32,128]{2,1,0:T(8,128)(2,1)}), bf16[16,32,128]{2,1,0:T(8,128)(2,1)S(1)}, u32[]{:S(2)}, u32[]{:S(2)}) %all-to-all-start) | async-done | bytes 131104 | tf_op jit(solution)/shard_map/all_to_all | solution.py:122
  113.5 5.0 %fusion.39 = (f32[32]{0:T(128)S(1)}, f32[32,2048]{1,0:T(8,128)S(1)}) fusion(bf16[2048,2048]{1,0:T(8,128)(2,1)} %param.23, bf16[32,2048]{1,0:T(8,128)(2,1)} %param.22, bf16[16,32,128]{2,1,0:T(8,128)(2,1)S(1)} %all-to-all-done), kind=kOutput, calls=%fused_computation.88 | convolution fusion | flops 268632032 | bytes 8913024 | tf_op jit(solution)/shard_map/dot_general | solution.py:123
  119.1 46.6 %all_to_all.38 = bf16[16,8,2048]{2,1,0:T(8,128)(2,1)S(1)} all-to-all(bf16[16,8,2048]{2,1,0:T(8,128)(2,1)S(1)} %fusion.21), channel_id=1, replica_groups=mesh['sp'=16,'tp'=16] {'sp'}, dimensions={0} | all-to-all | bytes 1048576 | tf_op jit(solution)/shard_map/all_to_all | solution.py:146
  166.5 187.3 %all_to_all.39 = bf16[16,128,2048]{2,1,0:T(8,128)(2,1)S(1)} all-to-all(bf16[16,128,2048]{2,1,0:T(8,128)(2,1)S(1)} %bitcast.91), channel_id=1, replica_groups=mesh['sp'=16,'tp'=16] {'tp'}, dimensions={0} | all-to-all | bytes 16777216 | tf_op jit(solution)/shard_map/all_to_all | solution.py:149
  353.7 3.2 copy-done.1
  357.0 3.8 fusion.25
  360.7 16.8 %convolution_convert_fusion = bf16[2048,2048]{1,0:T(8,128)(2,1)} fusion(bf16[2048,2048]{1,0:T(8,128)(2,1)} %bitcast.93, f32[2048,256]{1,0:T(8,128)} %fusion.25, bf16[1,256,2048]{2,1,0:T(8,128)(2,1)S(1)} %copy-done, bf16[1,2048,256]{2,1,0:T(8,128)(2,1)} %param.28), kind=kOutput, calls=%fused_computation.27 | convolution fusion | flops 4302307328 | bytes 20971520 | tf_op jit(solution)/shard_map/dot_general | solution.py:154
  377.6 66.7 %reduce-scatter.2.cloned.1.call-done = bf16[128,2048]{1,0:T(8,128)(2,1)} async-done(((bf16[2048,2048]{1,0:T(8,128)(2,1)}), bf16[128,2048]{1,0:T(8,128)(2,1)}) %reduce-scatter.2.cloned.1.call-update) | async-done | bytes 524304 | tf_op jit(solution)/shard_map/reduce_scatter | solution.py:153
  444.3 7.3 %all-to-all-start.3 = ((bf16[16,8,2048]{2,1,0:T(8,128)(2,1)}), bf16[16,8,2048]{2,1,0:T(8,128)(2,1)S(1)}, u32[]{:S(2)}, u32[]{:S(2)}) async-start(bf16[16,8,2048]{2,1,0:T(8,128)(2,1)} %bitcast.96), calls=%async_computation.4 | async-start | bytes 1048576 | tf_op jit(solution)/shard_map/all_to_all | solution.py:160
  451.8 8.6 %all-to-all-done.3 = bf16[16,8,2048]{2,1,0:T(8,128)(2,1)S(1)} async-done(((bf16[16,8,2048]{2,1,0:T(8,128)(2,1)}), bf16[16,8,2048]{2,1,0:T(8,128)(2,1)S(1)}, u32[]{:S(2)}, u32[]{:S(2)}) %all-to-all-start.3) | async-done | bytes 524320 | tf_op jit(solution)/shard_map/all_to_all | solution.py:160
  460.3 0.7 gather_fusion
  461.4 0.7 multiply_reduce_fusion
  (116 shorter events, 14.6 us)
Async XLA Ops:
  6.5 354.2 %copy-start = (bf16[1,256,2048]{2,1,0:T(8,128)(2,1)S(1)}, bf16[1,256,2048]{2,1,0:T(8,128)(2,1)}, u32[]{:S(2)}) copy-start(bf16[1,256,2048]{2,1,0:T(8,128)(2,1)} %param.29) | copy-start | bytes 3145732
  6.5 62.7 %all-gather.2.cloned.1.call-start = ((), (), s32[]{:S(2)}) async-start(), calls=%async_computation.5 | async-start | bytes 4456448 | tf_op jit(solution)/shard_map/all_gather | solution.py:18
  73.1 23.8 %copy-start.4 = (f32[128]{0:T(128)S(1)}, f32[128]{0:T(128)}, u32[]{:S(2)}) copy-start(f32[128]{0:T(128)} %param.21) | copy-start | bytes 1540
  97.7 15.8 %all-to-all-start = ((bf16[16,32,128]{2,1,0:T(8,128)(2,1)}), bf16[16,32,128]{2,1,0:T(8,128)(2,1)S(1)}, u32[]{:S(2)}, u32[]{:S(2)}) async-start(bf16[16,32,128]{2,1,0:T(8,128)(2,1)} %bitcast.16), calls=%async_computation | async-start | bytes 262144 | tf_op jit(solution)/shard_map/all_to_all | solution.py:122
  104.8 13.9 %copy-start.2 = (f32[2048]{0:T(1024)S(1)}, f32[2048]{0:T(1024)}, u32[]{:S(2)}) copy-start(f32[2048]{0:T(1024)} %param.24) | copy-start | bytes 24580
  104.8 339.4 %reduce-scatter.2.cloned.1.call-start = ((), (), s32[]{:S(2)}) async-start(), calls=%async_computation.6 | async-start | bytes 8912896 | tf_op jit(solution)/shard_map/reduce_scatter | solution.py:153
  166.5 190.5 %copy-start.5 = (bf16[1,2048,256]{2,1,0:T(8,128)(2,1)S(1)}, bf16[1,2048,256]{2,1,0:T(8,128)(2,1)}, u32[]{:S(2)}) copy-start(bf16[1,2048,256]{2,1,0:T(8,128)(2,1)} %param.27) | copy-start | bytes 3145732
  353.7 3.2 copy-start.1
  377.6 74.1 %copy-start.3 = (f32[32,2]{0,1:T(2,128)S(1)}, f32[32,2]{0,1:T(2,128)}, u32[]{:S(2)}) copy-start(f32[32,2]{0,1:T(2,128)} %param.26) | copy-start | bytes 772
  444.3 16.1 %all-to-all-start.3 = ((bf16[16,8,2048]{2,1,0:T(8,128)(2,1)}), bf16[16,8,2048]{2,1,0:T(8,128)(2,1)S(1)}, u32[]{:S(2)}, u32[]{:S(2)}) async-start(bf16[16,8,2048]{2,1,0:T(8,128)(2,1)} %bitcast.96), calls=%async_computation.4 | async-start | bytes 1048576 | tf_op jit(solution)/shard_map/all_to_all | solution.py:160
Sparse Core Ops, SparseCore 0:
  9.8 59.4 all-gather.1
  377.7 66.4 reduce-scatter.1
